TPU v7x, 32 devices: a whole 2x2x4 slice. The times are simulated.
32 devices in a mesh: kv: 16 (over z, y, x), tp: 2 (over core).
Axes of the slice: x: 2, y: 2, z: 4, core: 2. Of those that a mesh axis runs over, the one named last changes fastest.
Arguments:
- hidden_in: bfloat16 [8, 1024], P(None, 'tp'), may hold values from -18 to 18, as said below
- input_gain: float32 [1024], P('tp'), may hold values from 0.1 to 1.9
- down_query: bfloat16 [1024, 256], P('tp'), may hold values from -0.1875 to 0.1875
- down_latent: bfloat16 [1024, 256], P('tp'), may hold values from -0.1875 to 0.1875
- down_rope: bfloat16 [1024, 64], P('tp'), may hold values from -0.1875 to 0.1875
- query_gain: float32 [256], replicated, may hold values from 0.1 to 1.9
- latent_gain: float32 [256], replicated, may hold values from 0.1 to 1.9
- up_query: bfloat16 [256, 8, 128], P(None, 'tp'), may hold values from -0.375 to 0.375
- up_rope: bfloat16 [256, 8, 64], P(None, 'tp'), may hold values from -0.375 to 0.375
- key_up: bfloat16 [256, 8, 128], P(None, 'tp'), may hold values from -0.375 to 0.375
- value_up: bfloat16 [256, 8, 128], P(None, 'tp'), may hold values from -0.375 to 0.375
- out_proj: bfloat16 [1024, 1024], P('tp', 'kv'), may hold values from -2 to 2, as said below
- output_gain: float32 [1024], P('kv'), may hold values from 0.1 to 1.9
- latent_cache: bfloat16 [8, 4096, 256], P(None, ('kv', 'tp')), may hold values from -6 to 6
- rope_cache: bfloat16 [8, 4096, 64], P(None, ('kv', 'tp')), may hold values from -6 to 6
- lengths: int32 [8], replicated, may hold values from 1 to 4096, as said below
Outputs:
- mixed: bfloat16 [8, 1024], P(None, 'kv')
Inputs may be any that keep to these rules, and one draw needn't show every extreme that they name: Each length lies between 1 and 4096; in every draw some sequence has exactly 4096 and some exactly 1; lengths are heavily skewed toward short ones. `hidden_in`: activations whose size differs strongly between blocks of 64 features, by sequence. `out_proj`: output projection whose columns differ strongly in size.
All inputs are finite; a program needn't handle non-finite values.
Results may differ from a plain program's by a relative error of at most 0.015.
Values may be sent and summed in bfloat16 or wider, within the bound.
A program may use at most 128 MiB of HBM per device.

v0:
```python
import math

import jax
import jax.numpy as jnp
from jax import lax
from jax.sharding import PartitionSpec as P

D = 1024
DN = 128
DR = 64


THETA = 10000.0
EPSILON = 1e-06


def combined_all(value, axis, join):
    pieces = jax.tree.map(lambda part: lax.all_gather(part, axis), value)
    head = jax.tree.map(lambda part: part[0], pieces)
    tail = jax.tree.map(lambda part: part[1:], pieces)
    total, _ = lax.scan(lambda total, share: (join(total, share), None), head, tail)
    return total


def rotate(values, angles):
    half_width = values.shape[-1] // 2
    first_half = values[..., :half_width]
    second_half = values[..., half_width:]
    cosine = jnp.cos(angles)
    sine_part = jnp.sin(angles)
    return jnp.concatenate(
        [
            first_half * cosine - second_half * sine_part,
            second_half * cosine + first_half * sine_part,
        ],
        axis=-1,
    )


def angles_for(positions, rot_width):
    inverse = 1.0 / THETA ** (jnp.arange(0, rot_width, 2, dtype=jnp.float32) / rot_width)
    return positions[:, None] * inverse[None, :]


def normed(values, gain_row):
    return (
        values
        * lax.rsqrt(jnp.mean(values * values, axis=-1, keepdims=True) + EPSILON)
        * gain_row.astype(jnp.float32)
    )


def combine(earlier, later):
    highest = jnp.maximum(earlier[0], later[0])
    from_early = jnp.exp(earlier[0] - highest)
    from_late = jnp.exp(later[0] - highest)
    return (
        highest,
        earlier[1] * from_early + later[1] * from_late,
        earlier[2] * from_early[..., None] + later[2] * from_late[..., None],
    )


def shards(
    hidden_in,
    input_gain,
    down_query,
    down_latent,
    down_rope,
    query_gain,
    latent_gain,
    up_query,
    up_rope,
    key_up,
    value_up,
    out_proj,
    output_gain,
    latent_cache,
    rope_cache,
    lengths,
):
    floats = hidden_in.astype(jnp.float32)
    scaled = (floats * input_gain.astype(jnp.float32)).astype(jnp.bfloat16)
    local_sq = jnp.sum(floats * floats, axis=1)
    part_query = jnp.dot(scaled, down_query, preferred_element_type=jnp.float32)
    part_latent = jnp.dot(scaled, down_latent, preferred_element_type=jnp.float32)
    part_rope = jnp.dot(scaled, down_rope, preferred_element_type=jnp.float32)
    total_sq = lax.psum(local_sq, "tp")
    query_low, latent_low, rope_low = lax.psum((part_query, part_latent, part_rope), "tp")
    inv_rms = lax.rsqrt(total_sq / D + EPSILON)[:, None]
    query_low = query_low * inv_rms
    latent_low = latent_low * inv_rms
    rope_low = rope_low * inv_rms
    positions = lengths.astype(jnp.float32)
    query_normed = normed(query_low, query_gain).astype(jnp.bfloat16)
    query_nope = jnp.einsum(
        "bq,qhd->bhd", query_normed, up_query, preferred_element_type=jnp.float32
    ).astype(jnp.bfloat16)
    query_rope = jnp.einsum(
        "bq,qhr->bhr", query_normed, up_rope, preferred_element_type=jnp.float32
    )
    query_rope = rotate(query_rope, angles_for(positions, DR)[:, None, :]).astype(jnp.bfloat16)
    latent_heads = jnp.einsum(
        "bhd,chd->bhc", query_nope, key_up, preferred_element_type=jnp.float32
    ).astype(jnp.bfloat16)
    latent_query, rope_query = (
        lax.all_gather(latent_heads, "tp", axis=1, tiled=True),
        lax.all_gather(query_rope, "tp", axis=1, tiled=True),
    )
    latent_new = normed(latent_low, latent_gain).astype(jnp.bfloat16)
    rope_new = rotate(rope_low, angles_for(positions, DR)).astype(jnp.bfloat16)
    span_len = latent_cache.shape[1]
    offset = lax.axis_index(("kv", "tp")) * span_len
    places = offset + jnp.arange(span_len, dtype=jnp.int32)
    usable = (places[None, :] < lengths[:, None])[:, None, :]
    factor = 1.0 / math.sqrt(DN + DR)
    scores = (
        jnp.einsum("bhc,bpc->bhp", latent_query, latent_cache, preferred_element_type=jnp.float32)
        + jnp.einsum("bhr,bpr->bhp", rope_query, rope_cache, preferred_element_type=jnp.float32)
    ) * factor
    scores = jnp.where(usable, scores, -1e30)
    local_top = jnp.max(scores, axis=-1)
    weights = jnp.where(usable, jnp.exp(scores - local_top[..., None]), 0.0)
    local_mass = jnp.sum(weights, axis=-1)
    local_sum = jnp.einsum(
        "bhp,bpc->bhc",
        weights.astype(jnp.bfloat16),
        latent_cache,
        preferred_element_type=jnp.float32,
    )
    highest, total_mass, summed = combined_all(
        (local_top, local_mass, local_sum), ("kv", "tp"), combine
    )
    latent_wide = latent_new.astype(jnp.float32)
    new_score = (
        jnp.sum(latent_query.astype(jnp.float32) * latent_wide[:, None, :], axis=-1)
        + jnp.sum(
            rope_query.astype(jnp.float32) * rope_new.astype(jnp.float32)[:, None, :], axis=-1
        )
    ) * factor
    final_top = jnp.maximum(highest, new_score)
    keep_old = jnp.exp(highest - final_top)
    fresh_weight = jnp.exp(new_score - final_top)
    total_mass = total_mass * keep_old + fresh_weight
    summed = summed * keep_old[..., None] + fresh_weight[..., None] * latent_wide[:, None, :]
    attended = (summed / total_mass[..., None]).astype(jnp.bfloat16)
    heads_dev = value_up.shape[1]
    own_heads = lax.dynamic_slice_in_dim(attended, lax.axis_index("tp") * heads_dev, heads_dev, 1)
    values_out = jnp.einsum(
        "bhc,chv->bhv", own_heads, value_up, preferred_element_type=jnp.float32
    ).astype(jnp.bfloat16)
    flattened = values_out.reshape(values_out.shape[0], heads_dev * values_out.shape[2])
    out_part = jnp.dot(flattened, out_proj, preferred_element_type=jnp.float32)
    out_cols = lax.psum(out_part, "tp")
    out_sq = lax.psum(jnp.sum(out_cols * out_cols, axis=1), "kv")
    out_rms = lax.rsqrt(out_sq / D + EPSILON)[:, None]
    return (out_cols * out_rms * output_gain.astype(jnp.float32)).astype(jnp.bfloat16)


def solution(mesh):
    in_specs = (
        P(None, "tp"),
        P("tp"),
        P("tp", None),
        P("tp", None),
        P("tp", None),
        P(),
        P(),
        P(None, "tp", None),
        P(None, "tp", None),
        P(None, "tp", None),
        P(None, "tp", None),
        P("tp", "kv"),
        P("kv"),
        P(None, ("kv", "tp"), None),
        P(None, ("kv", "tp"), None),
        P(),
    )
    out_specs = P(None, "kv")
    return jax.shard_map(shards, mesh=mesh, in_specs=in_specs, out_specs=out_specs, check_vma=False)
```

profile of v0, /device:TPU:0, one launch (start us, length us, event | category | flops | bytes accessed | tf_op | source)
XLA Modules:
  0.0 160.4 jit_solution(5844168285014857857)
XLA Ops:
  6.6 0.7 convert_element_type.67
  7.3 0.7 broadcast_compare_fusion
  8.0 0.8 fusion.23
  8.8 1.0 fusion.38
  9.8 1.1 fusion.42
  11.0 1.1 fusion.40
  12.1 3.8 %all-reduce = (f32[8,256]{1,0:T(8,128)S(1)}, f32[8,256]{1,0:T(8,128)S(1)}, f32[8]{0:T(128)S(1)}, f32[8,64]{1,0:T(8,128)S(1)}) all-reduce(f32[8,256]{1,0:T(8,128)S(1)} %fusion.42, f32[8,256]{1,0:T(8,128)S(1)} %fusion.40, f32[8]{0:T(128)S(1)} %fusion.23, f32[8,64]{1,0:T(8,128)S(1)} %fusion.38), channel_id=1, replica_groups=mesh['kv'=16,'tp'=2] {'tp'}, use_global_device_ids=true, to_apply=%region_0.0 | all-reduce | flops 4616 | bytes 36928 | tf_op jit(solution)/shard_map/psum | solution.py:89
  16.0 0.2 multiply_reduce_fusion.2
  16.1 0.1 subtract_convert_fusion.1
  16.3 1.1 fusion.51
  17.4 0.1 pad_maximum_fusion
  17.5 1.8 %all_gather.25 = bf16[8,8,64]{2,0,1:T(8,128)(2,1)S(1)} all-gather(bf16[8,4,64]{2,0,1:T(8,128)(2,1)S(1)} %pad_maximum_fusion), channel_id=1, replica_groups=mesh['kv'=16,'tp'=2] {'tp'}, dimensions={1}, use_global_device_ids=true | all-gather | bytes 12288 | tf_op jit(solution)/shard_map/all_gather | solution.py:108
  19.4 1.4 fusion.5
  20.7 1.8 %all_gather.24 = bf16[8,8,256]{2,0,1:T(8,128)(2,1)S(1)} all-gather(bf16[8,4,256]{2,0,1:T(8,128)(2,1)S(1)} %fusion.5), channel_id=1, replica_groups=mesh['kv'=16,'tp'=2] {'tp'}, dimensions={1}, use_global_device_ids=true | all-gather | bytes 49152 | tf_op jit(solution)/shard_map/all_gather | solution.py:107
  22.6 0.2 fusion.15
  22.8 0.2 fusion.58
  23.0 0.9 fusion.24
  23.9 43.4 %all-gather = f32[256,8]{1,0:T(8,128)S(1)} all-gather(f32[8,8]{1,0:T(8,128)S(1)} %get-tuple-element.80), channel_id=2, replica_groups=mesh['kv'=16,'tp'=2] {'kv','tp'}, dimensions={0}, use_global_device_ids=true | all-gather | bytes 8448 | tf_op jit(solution)/shard_map/all_gather | solution.py:18
  67.3 0.2 fusion.19
  67.4 37.0 %all-gather.1 = f32[256,8]{1,0:T(8,128)S(1)} all-gather(f32[8,8]{1,0:T(8,128)S(1)} %fusion.19), channel_id=3, replica_groups=mesh['kv'=16,'tp'=2] {'kv','tp'}, dimensions={0}, use_global_device_ids=true | all-gather | bytes 8448 | tf_op jit(solution)/shard_map/all_gather | solution.py:18
  104.9 0.8 slice.50
  105.7 1.5 slice-done
  107.3 4.1 %while.14 = (s32[]{:T(128)}, f32[8,8]{1,0:T(8,128)S(1)}, f32[8,8]{1,0:T(8,128)S(1)}, f32[8,8,256]{2,1,0:T(8,128)S(1)}, f32[31,8,8]{2,1,0:T(8,128)S(1)}, /*index=...) while((s32[]{:T(128)}, f32[8,8]{1,0:T(8,128)S(1)}, f32[8,8]{1,0:T(8,128)S(1)}, ...), condition=%wide.region_7.8_spmd, body=%wide.region_6.0_spmd.sunk | while | flops 49538 | bytes 199269 | solution.py:21
  107.3 0.1 fusion.70
  107.7 0.1 fusion.70
  108.0 0.1 fusion.70
  108.4 0.1 fusion.70
  111.6 0.3 fusion.7
  111.9 2.5 %psum.46 = f32[8,64]{1,0:T(8,128)S(1)} all-reduce(f32[8,64]{1,0:T(8,128)S(1)} %fusion.7), channel_id=1, replica_groups=mesh['kv'=16,'tp'=2] {'tp'}, use_global_device_ids=true, to_apply=%region_13.14 | all-reduce | flops 512 | bytes 4096 | tf_op jit(solution)/shard_map/psum | solution.py:154
  114.4 0.1 multiply_reduce_fusion.4
  114.5 38.3 %psum.47 = f32[8]{0:T(128)S(1)} all-reduce(f32[8]{0:T(128)S(1)} %multiply_reduce_fusion.4), channel_id=1, replica_groups=mesh['kv'=16,'tp'=2] {'kv'}, use_global_device_ids=true, to_apply=%region_15.16 | all-reduce | flops 8 | bytes 64 | tf_op jit(solution)/shard_map/psum | solution.py:155
  152.9 0.7 multiply_convert_fusion.2
  (96 shorter events, 3.7 us)
Async XLA Ops:
  6.5 16.0 %copy-start = (bf16[8,128,256]{2,1,0:T(8,128)(2,1)S(1)}, bf16[8,128,256]{2,1,0:T(8,128)(2,1)}, u32[]{:S(2)}) copy-start(bf16[8,128,256]{2,1,0:T(8,128)(2,1)} %param.31) | copy-start | bytes 1572868
  6.5 16.2 %copy-start.1 = (bf16[8,128,64]{1,2,0:T(8,128)(2,1)S(1)}, bf16[8,128,64]{1,2,0:T(8,128)(2,1)}, u32[]{:S(2)}) copy-start(bf16[8,128,64]{1,2,0:T(8,128)(2,1)} %param.32) | copy-start | bytes 393220
  6.5 98.1 %copy-start.2 = (f32[256]{0:T(256)S(1)}, f32[256]{0:T(256)}, u32[]{:S(2)}) copy-start(f32[256]{0:T(256)} %param.24) | copy-start | bytes 3076
  6.5 98.3 %all-gather.5.cloned.1.call-start = ((), (), s32[]{:S(2)}) async-start(), calls=%async_computation | async-start | bytes 2162688 | tf_op jit(solution)/shard_map/all_gather | solution.py:18
  105.7 1.6 slice-start
  105.7 5.9 %copy-start.4 = (bf16[256,4,128]{2,1,0:T(4,128)(2,1)S(1)}, bf16[256,4,128]{2,1,0:T(4,128)(2,1)}, u32[]{:S(2)}) copy-start(bf16[256,4,128]{2,1,0:T(4,128)(2,1)} %param.28) | copy-start | bytes 786436
  105.7 5.9 %copy-start.5 = (bf16[512,64]{0,1:T(8,128)(2,1)S(1)}, bf16[512,64]{0,1:T(8,128)(2,1)}, u32[]{:S(2)}) copy-start(bf16[512,64]{0,1:T(8,128)(2,1)} %param.29) | copy-start | bytes 196612
  105.7 47.2 %copy-start.3 = (f32[64]{0:T(128)S(1)}, f32[64]{0:T(128)}, u32[]{:S(2)}) copy-start(f32[64]{0:T(128)} %param.30) | copy-start | bytes 772
Sparse Core Ops, SparseCore 0:
  24.0 58.7 all-gather.4
where the time goes:
time: 161 us; the launch traced here: 160 us
  blocking collectives  129 us (80%)
  between operations  13.6 us (8%)
  other arithmetic  7.42 us (5%)
  matrix products  7.37 us (5%)
  local copies, waits for them, and re-layouts  2.62 us (2%)
    all_gather x2, blocking collectives, combined_all(): pieces = jax.tree.map(lambda part: lax.all_gather(part, axis), value)  80.4 us
    psum x1, blocking collectives, shards(): out_sq = lax.psum(jnp.sum(out_cols * out_cols, axis=1), 'kv')  38.3 us
    psum x1, blocking collectives, shards(): lax.psum((part_query, part_latent, part_rope), 'tp')  3.76 us
  transfers between devices with their start and end apart: 1, of which 0 were waited for; matrix products, arithmetic and copies ran while one was open for 0% of the time, Pallas kernels for 0%

commit v1 on v0

v1 whole, which is shorter than its diff:
```python
import functools
import math

import jax
import jax.numpy as jnp
import numpy as np
from jax import lax
from jax.experimental import pallas as pl
from jax.experimental.pallas import tpu as pltpu
from jax.sharding import PartitionSpec as P

THETA = 10000.0
EPSILON = 1e-06
MESH = pl.DeviceIdType.MESH
F32 = jnp.float32
BF16 = jnp.bfloat16
NT = (((1,), (1,)), ((), ()))


def iota(shape, dim):
    return lax.broadcasted_iota(jnp.int32, shape, dim)


def dot(a, b):
    return jnp.dot(a, b, preferred_element_type=F32)


def dot_nt(a, b):
    return lax.dot_general(a, b, NT, preferred_element_type=F32)


def sin_cos(x):
    turns = jnp.floor(x * (1.0 / (2 * math.pi)) + 0.5)
    r = (x - turns * 6.28125) - turns * (2 * math.pi - 6.28125)
    r2 = r * r
    s = jnp.full_like(x, 1.0)
    for n in (15, 13, 11, 9, 7, 5, 3):
        s = 1.0 - s * r2 * (1.0 / (n * (n - 1)))
    c = jnp.full_like(x, 1.0)
    for n in (18, 16, 14, 12, 10, 8, 6, 4, 2):
        c = 1.0 - c * r2 * (1.0 / (n * (n - 1)))
    return s * r, c


def turn(v, cosine, sine):
    half = v.shape[-1] // 2
    swapped = jnp.concatenate([-v[:, half:], v[:, :half]], axis=1)
    return v * cosine + swapped * sine


def normed(v, gain):
    return v * lax.rsqrt(jnp.mean(v * v, axis=-1, keepdims=True) + EPSILON) * gain


def kernel(
    K,
    T,
    lengths,
    inverse,
    hidden_h,
    gain_h,
    dq_h,
    dl_h,
    dr_h,
    qg_h,
    lg_h,
    uq_h,
    ur_h,
    ku_h,
    vu_h,
    op_h,
    og_h,
    lat_h,
    rope_h,
    out,
    hidden,
    gain,
    dq,
    dl,
    dr,
    qg,
    lg,
    uq,
    ur,
    ku,
    vu,
    og,
    lat,
    rope,
    rx1,
    rx2,
    rxp,
    tx3,
    rx3,
    tx4,
    rx4,
    rx6,
    spread,
    load_sem,
    s1,
    r1,
    s2,
    r2,
    sp,
    rp,
    s3,
    r3,
    s4,
    r4,
    s6,
    r6,
):
    N = K * T
    B = hidden.shape[0]
    width = hidden.shape[1] * T
    QR = dq.shape[1]
    KR = dl.shape[1]
    DR = dr.shape[0]
    Hd = uq.shape[0] // QR
    H = Hd * T
    DN = uq.shape[1]
    span = lat.shape[1]
    rows = rx3.shape[1]
    owners = tx3.shape[0]
    k = lax.axis_index("kv")
    t = lax.axis_index("tp")
    me = k * T + t
    factor = 1.0 / math.sqrt(DN + DR)

    def place(d):
        return (lax.div(d, T), lax.rem(d, T))

    def slot_of(d):
        first = lax.div(d, T) * rows
        return lax.div(lax.div(first, Hd) * H + lax.rem(d, T) * Hd + lax.rem(first, Hd), rows)

    everyone_owns = owners == N

    def if_owner(d, fn):
        if everyone_owns:
            fn()
        else:
            pl.when(lax.div(d, T) * T * rows < B * H)(fn)

    barrier = pltpu.get_barrier_semaphore()

    def greet(i, carry):
        pl.semaphore_signal(barrier, inc=1, device_id=place(lax.rem(me + i, N)), device_id_type=MESH)
        return carry

    lax.fori_loop(1, N, greet, 0)

    pairs = (
        (hidden_h, hidden), (gain_h, gain), (dq_h, dq), (dl_h, dl), (dr_h, dr),
        (uq_h, uq), (ur_h, ur), (ku_h, ku), (qg_h, qg), (lg_h, lg),
        (op_h, rxp.at[t]), (lat_h, lat), (rope_h, rope), (vu_h, vu), (og_h, og),
    )
    loads = [pltpu.make_async_copy(a, b, load_sem.at[i]) for i, (a, b) in enumerate(pairs)]
    for load in loads:
        load.start()

    spread[...] = jnp.where(
        lax.div(iota((QR, QR * Hd), 1), Hd) == iota((QR, QR * Hd), 0), 1.0, 0.0
    ).astype(BF16)
    own_rows = iota((B * H, QR * Hd), 0)
    own_mask = (lax.rem(own_rows, H) - t * Hd) == lax.rem(iota((B * H, QR * Hd), 1), Hd)

    def angles(n, per):
        row = lax.div(iota((n, DR), 0), per)
        position = jnp.zeros((n, DR), F32)
        for b in range(B):
            position = jnp.where(row == b, lengths[b].astype(F32), position)
        return sin_cos(position * inverse[...])

    sine8, cosine8 = angles(B, 1)
    sine_all, cosine_all = angles(B * H, H)

    for load in loads[:5]:
        load.wait()
    floats = hidden[...].astype(F32)
    scaled = (floats * gain[...]).astype(BF16)
    low = rx1.at[t]
    low[:, :QR] = dot(scaled, dq[...])
    low[:, QR : QR + KR] = dot(scaled, dl[...])
    low[:, QR + KR : QR + KR + DR] = dot_nt(scaled, dr[...])
    low[:, QR + KR + DR :] = jnp.broadcast_to(
        jnp.sum(floats * floats, axis=1, keepdims=True), (B, rx1.shape[2] - QR - KR - DR)
    )
    pl.semaphore_wait(barrier, N - 1)

    def swap(buffer, send, recv):
        copies = []
        for i in range(1, T):
            peer = lax.rem(t + i, T)
            copies.append(
                pltpu.make_async_remote_copy(
                    src_ref=buffer.at[t],
                    dst_ref=buffer.at[t],
                    send_sem=send.at[i],
                    recv_sem=recv.at[i],
                    device_id=(k, peer),
                    device_id_type=MESH,
                )
            )
        for copy in copies:
            copy.start()
        return copies

    copies1 = swap(rx1, s1, r1)
    for load in loads[5:]:
        load.wait()
    for copy in copies1:
        copy.wait()
    total = rx1[0]
    for i in range(1, T):
        total = total + rx1[i]
    inv_rms = lax.rsqrt(total[:, QR + KR + DR : QR + KR + DR + 1] / width + EPSILON)
    total = total * inv_rms
    query_normed = normed(total[:, :QR], qg[...]).astype(BF16)
    latent_new = normed(total[:, QR : QR + KR], lg[...]).astype(BF16).astype(F32)
    rope_new = turn(total[:, QR + KR : QR + KR + DR], cosine8, sine8).astype(BF16).astype(F32)

    wide = dot(query_normed, spread[...])
    wide = jnp.concatenate(
        [jnp.broadcast_to(wide[b : b + 1, :], (H, QR * Hd)) for b in range(B)], axis=0
    )
    wide = jnp.where(own_mask, wide, 0.0).astype(BF16)
    query_nope = dot(wide, uq[...]).astype(BF16)
    roped = dot_nt(query_normed, ur[...])
    roped = jnp.concatenate(
        [jnp.broadcast_to(roped[b : b + 1, :], (H, Hd * DR)) for b in range(B)], axis=0
    )
    head = lax.rem(iota((B * H, DR), 0), H) - t * Hd
    query_rope = jnp.zeros((B * H, DR), F32)
    for h in range(Hd):
        query_rope = jnp.where(head == h, roped[:, h * DR : (h + 1) * DR], query_rope)
    query_rope = turn(query_rope, cosine_all, sine_all)
    tall = jnp.where(own_mask, dot_nt(query_nope, ku[...]), 0.0).astype(BF16)
    queries = rx2.at[t]
    queries[:, :KR] = dot_nt(tall, spread[...]).astype(BF16)
    queries[:, KR : KR + DR] = query_rope.astype(BF16)
    queries[:, KR + DR :] = jnp.zeros((B * H, rx2.shape[2] - KR - DR), BF16)
    copies2 = swap(rx2, s2, r2)
    copies_p = swap(rxp, sp, rp)
    for copy in copies2:
        copy.wait()
    query = rx2[0].astype(F32)
    for i in range(1, T):
        query = query + rx2[i].astype(F32)

    offset = me * span
    lane = iota((H, span), 1) + offset
    mark = iota((H, 128), 1)
    first = me == 0
    for b in range(B):
        q = query[b * H : (b + 1) * H]
        qb = q.astype(BF16)
        usable = lane < lengths[b]
        scores = (
            dot_nt(qb[:, :KR], lat[b]) + dot(qb[:, KR : KR + DR], rope[b])
        ) * factor
        scores = jnp.where(usable, scores, -1e30)
        new_score = (
            jnp.sum(q[:, :KR] * latent_new[b : b + 1], axis=1, keepdims=True)
            + jnp.sum(q[:, KR : KR + DR] * rope_new[b : b + 1], axis=1, keepdims=True)
        ) * factor
        new_score = jnp.where(first, new_score, -1e30)
        top = jnp.maximum(jnp.max(scores, axis=1, keepdims=True), new_score)
        weights = jnp.where(usable, jnp.exp(scores - top), 0.0)
        fresh = jnp.where(first, jnp.exp(new_score - top), 0.0)
        mass = jnp.sum(weights, axis=1, keepdims=True) + fresh
        summed = dot(weights.astype(BF16), lat[b]) + fresh * latent_new[b : b + 1]
        high = top.astype(BF16).astype(F32)
        middle = (top - high).astype(BF16).astype(F32)
        small = ((top - high) - middle).astype(BF16).astype(F32)
        mass_high = mass.astype(BF16).astype(F32)
        tail = jnp.where(
            mark == 0,
            high,
            jnp.where(
                mark == 1,
                middle,
                jnp.where(mark == 2, small, jnp.where(mark == 3, mass_high, mass - mass_high)),
            ),
        )
        block = jnp.concatenate([summed, tail], axis=1).astype(BF16)
        for j in range(H // rows):
            tx3[b * (H // rows) + j] = block[j * rows : (j + 1) * rows]

    def part(d):
        return pltpu.make_async_remote_copy(
            src_ref=tx3.at[slot_of(d)],
            dst_ref=rx3.at[me],
            send_sem=s3,
            recv_sem=r3,
            device_id=place(d),
            device_id_type=MESH,
        )

    def send3(i, carry):
        d = lax.rem(me + i, N)
        if_owner(d, part(d).start)
        return carry

    lax.fori_loop(1, N, send3, 0)

    mine = slot_of(me)

    def values(d):
        return pltpu.make_async_remote_copy(
            src_ref=tx4,
            dst_ref=rx4.at[mine],
            send_sem=s4,
            recv_sem=r4,
            device_id=place(d),
            device_id_type=MESH,
        )

    def own():
        rx3[me] = tx3[mine]
        pltpu.make_async_copy(rx3.at[pl.ds(0, N - 1)], rx3.at[pl.ds(0, N - 1)], r3).wait()
        parts = rx3[...].astype(F32)
        tail = parts[:, :, KR : KR + 128]
        top = tail[:, :, 0:1] + tail[:, :, 1:2] + tail[:, :, 2:3]
        highest = jnp.max(top, axis=0, keepdims=True)
        scale = jnp.exp(top - highest)
        mass = jnp.sum((tail[:, :, 3:4] + tail[:, :, 4:5]) * scale, axis=0)
        attended = jnp.sum(parts[:, :, :KR] * scale, axis=0) / mass
        attended = jnp.concatenate([attended, jnp.zeros((8 - rows, KR), F32)], axis=0)
        wide = dot(attended.astype(BF16), spread[...])
        head = lax.rem(k * rows + iota((8, KR * Hd), 0), Hd)
        wide = jnp.where(head == lax.rem(iota((8, KR * Hd), 1), Hd), wide, 0.0).astype(BF16)
        value = dot(wide, vu[...])[:rows].astype(BF16)
        tx4[...] = value
        rx4[mine] = value

        def send4(i, carry):
            values(lax.rem(me + i, N)).start()
            return carry

        lax.fori_loop(1, N, send4, 0)

    if_owner(me, own)
    for copy in copies_p:
        copy.wait()

    def arrived(n):
        pltpu.make_async_copy(rx4.at[pl.ds(0, n)], rx4.at[pl.ds(0, n)], r4).wait()

    if everyone_owns:
        arrived(owners - 1)
    else:
        owner = k * T * rows < B * H
        pl.when(owner)(lambda: arrived(owners - 1))
        pl.when(jnp.logical_not(owner))(lambda: arrived(owners))

    gathered = rx4[...].astype(F32).reshape(B, H, rx4.shape[2]).astype(BF16)
    out_cols = jnp.zeros(out.shape, F32)
    for i in range(T):
        flat = jnp.concatenate([gathered[:, i * Hd + h, :] for h in range(Hd)], axis=1)
        out_cols = out_cols + dot_nt(flat, rxp[i])
    squares = jnp.sum(out_cols * out_cols, axis=1, keepdims=True)
    diagonal = iota((B, 128), 0) == iota((B, 128), 1)
    rx6[k] = jnp.sum(jnp.where(diagonal, squares, 0.0), axis=0, keepdims=True)

    def norm_part(i):
        return pltpu.make_async_remote_copy(
            src_ref=rx6.at[k],
            dst_ref=rx6.at[k],
            send_sem=s6,
            recv_sem=r6,
            device_id=(lax.rem(k + i, K), t),
            device_id_type=MESH,
        )

    def send6(i, carry):
        norm_part(i).start()
        return carry

    lax.fori_loop(1, K, send6, 0)

    def sent3(i, carry):
        d = lax.rem(me + i, N)
        if_owner(d, part(d).wait_send)
        return carry

    def sent4(i, carry):
        values(lax.rem(me + i, N)).wait_send()
        return carry

    lax.fori_loop(1, N, sent3, 0)
    def left4():
        lax.fori_loop(1, N, sent4, 0)

    if_owner(me, left4)

    pltpu.make_async_copy(rx6.at[pl.ds(0, K - 1)], rx6.at[pl.ds(0, K - 1)], r6).wait()
    total = jnp.sum(rx6[...], axis=0)
    squares = jnp.sum(
        jnp.where(diagonal, jnp.broadcast_to(total, (B, 128)), 0.0), axis=1, keepdims=True
    )
    out[...] = (out_cols * lax.rsqrt(squares / width + EPSILON) * og[...]).astype(BF16)

    def sent6(i, carry):
        norm_part(i).wait_send()
        return carry

    lax.fori_loop(1, K, sent6, 0)


def shards(
    K, T, hidden_in, input_gain, down_query, down_latent, down_rope, query_gain, latent_gain,
    up_query, up_rope, key_up, value_up, out_proj, output_gain, latent_cache, rope_cache, lengths,
):
    B = hidden_in.shape[0]
    QR, Hd, DN = up_query.shape
    KR, DR, DV = key_up.shape[0], up_rope.shape[2], value_up.shape[2]
    H, N = Hd * T, K * T
    rows = max(1, B * Hd // K)
    owners = B * H // rows
    steps = np.arange(0, DR, 2, dtype=np.float64) / DR
    inverse = np.tile((1.0 / THETA**steps).astype(np.float32), 2)[None, :]
    flat = lambda w: w.reshape(w.shape[0] * w.shape[1], w.shape[2])
    row = lambda v: v.reshape(1, v.shape[0])
    arrays = (
        hidden_in, row(input_gain), down_query, down_latent, down_rope.T, row(query_gain),
        row(latent_gain), flat(up_query), flat(up_rope.transpose(1, 2, 0)), flat(key_up),
        flat(value_up), out_proj.T, row(output_gain), latent_cache,
        rope_cache.transpose(0, 2, 1),
    )
    vm = lambda a: pltpu.VMEM(a.shape, a.dtype)
    local = [vm(a) for i, a in enumerate(arrays) if i != 11]
    low = -(-(QR + KR + DR + 1) // 128) * 128
    wide = -(-(KR + DR) // 128) * 128
    dma = pltpu.SemaphoreType.DMA
    scratch = local + [
        pltpu.VMEM((T, B, low), F32),
        pltpu.VMEM((T, B * H, wide), BF16),
        pltpu.VMEM((T,) + out_proj.shape[::-1], BF16),
        pltpu.VMEM((owners, rows, KR + 128), BF16),
        pltpu.VMEM((N, rows, KR + 128), BF16),
        pltpu.VMEM((rows, DV), BF16),
        pltpu.VMEM((owners, rows, DV), BF16),
        pltpu.VMEM((K, 1, 128), F32),
        pltpu.VMEM((QR, QR * Hd), BF16),
        dma((len(arrays),)),
        dma((T,)), dma((T,)), dma((T,)), dma((T,)), dma((T,)), dma((T,)),
        dma, dma, dma, dma, dma, dma,
    ]
    return pl.pallas_call(
        functools.partial(kernel, K, T),
        out_shape=jax.ShapeDtypeStruct((B, out_proj.shape[1]), BF16),
        in_specs=[
            pl.BlockSpec(memory_space=pltpu.SMEM),
            pl.BlockSpec(memory_space=pltpu.VMEM),
        ]
        + [pl.BlockSpec(memory_space=pl.ANY)] * len(arrays),
        out_specs=pl.BlockSpec(memory_space=pltpu.VMEM),
        scratch_shapes=scratch,
        compiler_params=pltpu.CompilerParams(collective_id=0, has_side_effects=True),
    )(lengths, jnp.asarray(inverse), *arrays)


def solution(mesh):
    in_specs = (
        P(None, "tp"),
        P("tp"),
        P("tp", None),
        P("tp", None),
        P("tp", None),
        P(),
        P(),
        P(None, "tp", None),
        P(None, "tp", None),
        P(None, "tp", None),
        P(None, "tp", None),
        P("tp", "kv"),
        P("kv"),
        P(None, ("kv", "tp"), None),
        P(None, ("kv", "tp"), None),
        P(),
    )
    body = functools.partial(shards, mesh.shape["kv"], mesh.shape["tp"])
    return jax.shard_map(body, mesh=mesh, in_specs=in_specs, out_specs=P(None, "kv"), check_vma=False)
```

time: 161 us -> 28.2 us (0.18)
  blocking collectives: 129 us -> 0 us
  Pallas kernels: 0 us -> 26.7 us
  between operations: 13.6 us -> 0.01 us
  other arithmetic: 7.42 us -> 0 us
  matrix products: 7.37 us -> 0 us
    all_gather x4 -> x0, blocking collectives: 84 us -> none  [the longest x2 80.4 us: combined_all(): pieces = jax.tree.map(lambda part: lax.all_gather(part, axis), value)]
    psum x3 -> x0, blocking collectives: 44.6 us -> none  [the longest x1 38.3 us: shards(): out_sq = lax.psum(jnp.sum(out_cols * out_cols, axis=1), 'kv')]
    pallas_call x0 -> x1, Pallas kernels: none -> 26.7 us  [shards(): pl.pallas_call(functools.partial(kernel, K, T), out_shape=jax.ShapeDtypeS...]
    dot_general x9 -> x0, matrix products: 7.37 us -> none  [the longest x1 1.36 us: shards(): jnp.einsum('bhd,chd->bhc', query_nope, key_up, preferred_element_type=jnp...]
    add x64 -> x0, other arithmetic: 3.32 us -> none  [the longest x31 2.81 us: combine(): earlier[2] * from_early[..., None] + later[2] * from_late[..., None]]
    slice x7 -> x0, local copies, waits for them, and re-layouts: 2.41 us -> none  [the longest x4 1.56 us: combined_all(): tail = jax.tree.map(lambda part: part[1:], pieces)]
  transfers between devices with their start and end apart: 1 -> 0, of which waited for: 0 -> 0; matrix products, arithmetic and copies ran while one was open for 0% -> 0% of each run, Pallas kernels for 0% -> 0%
where the time goes in v1:
time: 28.2 us; the launch traced here: 28 us
  Pallas kernels  26.7 us (95%)
  local copies, waits for them, and re-layouts  1.26 us (4%)
    pallas_call x1, Pallas kernels, shards(): pl.pallas_call(functools.partial(kernel, K, T), out_shape=jax.ShapeDtypeS...  26.7 us
    unnamed x1, local copies, waits for them, and re-layouts  1.26 us

profile of v1, /device:TPU:0, one launch (start us, length us, event | category | flops | bytes accessed | tf_op | source)
XLA Modules:
  0.0 28.0 jit_solution(13760013167025470444)
XLA Ops:
  0.0 26.7 %shard_map.163 = bf16[8,64]{1,0:T(8,128)(2,1)} custom-call(s32[8]{0:T(128)} %lengths.1, f32[1,64]{1,0:T(1,128)} %constant.2.clone.inverse, bf16[8,512]{1,0:T(8,128)(2,1)} %hidden_h.1, f32[1,512]{1,0:T(1,128)} %bitcast.20, bf16[512,256]{1,0:T(8,128)(2,1)} %dq_h.1, bf16[512,256]{1,0:T(8,128)(2,1)} %dl_h.1, bf16[64,512]{1,0:T(8,128)(2,1)} %bitcast.18, ...), custom_call_target="tpu_custom_call" | custom-call | tf_op jit(solution)/shard_map/pallas_call | solution.py:450
  26.7 1.3 %copy.19 = bf16[8,64]{1,0:T(8,128)(2,1)} copy(bf16[8,64]{1,0:T(8,128)(2,1)} %shard_map.163) | data formatting | bytes 2048

commit v2 on v1

--- a/solution.py
+++ b/solution.py
@@ -55,8 +55,8 @@
 def kernel(
     K,
     T,
-    lengths,
-    inverse,
+    lengths_h,
+    inverse_h,
     hidden_h,
     gain_h,
     dq_h,
@@ -69,7 +69,6 @@
     ku_h,
     vu_h,
     op_h,
-    og_h,
     lat_h,
     rope_h,
     out,
@@ -84,7 +83,6 @@
     ur,
     ku,
     vu,
-    og,
     lat,
     rope,
     rx1,
@@ -96,6 +94,8 @@
     rx4,
     rx6,
     spread,
+    lengths,
+    inverse,
     load_sem,
     s1,
     r1,
@@ -127,33 +127,40 @@
     me = k * T + t
     factor = 1.0 / math.sqrt(DN + DR)
 
-    def place(d):
-        return (lax.div(d, T), lax.rem(d, T))
-
-    def slot_of(d):
-        first = lax.div(d, T) * rows
-        return lax.div(lax.div(first, Hd) * H + lax.rem(d, T) * Hd + lax.rem(first, Hd), rows)
+    def slot_of(kk, tt):
+        first = kk * rows
+        return lax.div(lax.div(first, Hd) * H + tt * Hd + lax.rem(first, Hd), rows)
 
     everyone_owns = owners == N
 
-    def if_owner(d, fn):
+    def if_owner(kk, fn):
         if everyone_owns:
             fn()
         else:
-            pl.when(lax.div(d, T) * T * rows < B * H)(fn)
+            pl.when(kk * T * rows < B * H)(fn)
 
     barrier = pltpu.get_barrier_semaphore()
 
-    def greet(i, carry):
-        pl.semaphore_signal(barrier, inc=1, device_id=place(lax.rem(me + i, N)), device_id_type=MESH)
-        return carry
-
-    lax.fori_loop(1, N, greet, 0)
+    def to_all(fn):
+        def chip(i, carry):
+            kk = k + i
+            kk = jnp.where(kk >= K, kk - K, kk)
+            for tt in range(T):
+                fn(kk, tt)
+            return carry
+
+        lax.fori_loop(K // 2, K, chip, 0)
+        lax.fori_loop(1, K // 2, chip, 0)
+        for i in range(1, T):
+            fn(k, lax.rem(t + i, T))
+
+    to_all(lambda kk, tt: pl.semaphore_signal(barrier, inc=1, device_id=(kk, tt), device_id_type=MESH))
 
     pairs = (
         (hidden_h, hidden), (gain_h, gain), (dq_h, dq), (dl_h, dl), (dr_h, dr),
         (uq_h, uq), (ur_h, ur), (ku_h, ku), (qg_h, qg), (lg_h, lg),
-        (op_h, rxp.at[t]), (lat_h, lat), (rope_h, rope), (vu_h, vu), (og_h, og),
+        (op_h, rxp.at[t]), (lat_h, lat), (rope_h, rope), (vu_h, vu),
+        (lengths_h, lengths), (inverse_h, inverse),
     )
     loads = [pltpu.make_async_copy(a, b, load_sem.at[i]) for i, (a, b) in enumerate(pairs)]
     for load in loads:
@@ -171,9 +178,6 @@
         for b in range(B):
             position = jnp.where(row == b, lengths[b].astype(F32), position)
         return sin_cos(position * inverse[...])
-
-    sine8, cosine8 = angles(B, 1)
-    sine_all, cosine_all = angles(B * H, H)
 
     for load in loads[:5]:
         load.wait()
@@ -186,6 +190,10 @@
     low[:, QR + KR + DR :] = jnp.broadcast_to(
         jnp.sum(floats * floats, axis=1, keepdims=True), (B, rx1.shape[2] - QR - KR - DR)
     )
+    for load in loads[-2:]:
+        load.wait()
+    sine8, cosine8 = angles(B, 1)
+    sine_all, cosine_all = angles(B * H, H)
     pl.semaphore_wait(barrier, N - 1)
 
     def swap(buffer, send, recv):
@@ -207,7 +215,7 @@
         return copies
 
     copies1 = swap(rx1, s1, r1)
-    for load in loads[5:]:
+    for load in loads[5:-2]:
         load.wait()
     for copy in copies1:
         copy.wait()
@@ -287,32 +295,27 @@
         for j in range(H // rows):
             tx3[b * (H // rows) + j] = block[j * rows : (j + 1) * rows]
 
-    def part(d):
+    def part(kk, tt):
         return pltpu.make_async_remote_copy(
-            src_ref=tx3.at[slot_of(d)],
+            src_ref=tx3.at[slot_of(kk, tt)],
             dst_ref=rx3.at[me],
             send_sem=s3,
             recv_sem=r3,
-            device_id=place(d),
+            device_id=(kk, tt),
             device_id_type=MESH,
         )
 
-    def send3(i, carry):
-        d = lax.rem(me + i, N)
-        if_owner(d, part(d).start)
-        return carry
-
-    lax.fori_loop(1, N, send3, 0)
-
-    mine = slot_of(me)
-
-    def values(d):
+    to_all(lambda kk, tt: if_owner(kk, lambda: part(kk, tt).start()))
+
+    mine = slot_of(k, t)
+
+    def values(kk, tt):
         return pltpu.make_async_remote_copy(
             src_ref=tx4,
             dst_ref=rx4.at[mine],
             send_sem=s4,
             recv_sem=r4,
-            device_id=place(d),
+            device_id=(kk, tt),
             device_id_type=MESH,
         )
 
@@ -334,13 +337,9 @@
         tx4[...] = value
         rx4[mine] = value
 
-        def send4(i, carry):
-            values(lax.rem(me + i, N)).start()
-            return carry
-
-        lax.fori_loop(1, N, send4, 0)
-
-    if_owner(me, own)
+        to_all(lambda kk, tt: values(kk, tt).start())
+
+    if_owner(k, own)
     for copy in copies_p:
         copy.wait()
 
@@ -379,33 +378,23 @@
 
     lax.fori_loop(1, K, send6, 0)
 
-    def sent3(i, carry):
-        d = lax.rem(me + i, N)
-        if_owner(d, part(d).wait_send)
-        return carry
-
-    def sent4(i, carry):
-        values(lax.rem(me + i, N)).wait_send()
-        return carry
-
-    lax.fori_loop(1, N, sent3, 0)
-    def left4():
-        lax.fori_loop(1, N, sent4, 0)
-
-    if_owner(me, left4)
+    def left(buffer, n, sem):
+        pltpu.make_async_copy(buffer.at[pl.ds(0, n)], buffer.at[pl.ds(0, n)], sem).wait()
+
+    if everyone_owns:
+        left(rx3, N - 1, s3)
+        left(rx4, N - 1, s4)
+    else:
+        to_all(lambda kk, tt: if_owner(kk, lambda: part(kk, tt).wait_send()))
+        if_owner(k, lambda: to_all(lambda kk, tt: values(kk, tt).wait_send()))
 
     pltpu.make_async_copy(rx6.at[pl.ds(0, K - 1)], rx6.at[pl.ds(0, K - 1)], r6).wait()
     total = jnp.sum(rx6[...], axis=0)
     squares = jnp.sum(
         jnp.where(diagonal, jnp.broadcast_to(total, (B, 128)), 0.0), axis=1, keepdims=True
     )
-    out[...] = (out_cols * lax.rsqrt(squares / width + EPSILON) * og[...]).astype(BF16)
-
-    def sent6(i, carry):
-        norm_part(i).wait_send()
-        return carry
-
-    lax.fori_loop(1, K, sent6, 0)
+    out[...] = out_cols * lax.rsqrt(squares / width + EPSILON)
+    left(rx6, K - 1, s6)
 
 
 def shards(
@@ -425,8 +414,7 @@
     arrays = (
         hidden_in, row(input_gain), down_query, down_latent, down_rope.T, row(query_gain),
         row(latent_gain), flat(up_query), flat(up_rope.transpose(1, 2, 0)), flat(key_up),
-        flat(value_up), out_proj.T, row(output_gain), latent_cache,
-        rope_cache.transpose(0, 2, 1),
+        flat(value_up), out_proj.T, latent_cache, rope_cache.transpose(0, 2, 1),
     )
     vm = lambda a: pltpu.VMEM(a.shape, a.dtype)
     local = [vm(a) for i, a in enumerate(arrays) if i != 11]
@@ -443,22 +431,21 @@
         pltpu.VMEM((owners, rows, DV), BF16),
         pltpu.VMEM((K, 1, 128), F32),
         pltpu.VMEM((QR, QR * Hd), BF16),
-        dma((len(arrays),)),
+        pltpu.SMEM(lengths.shape, lengths.dtype),
+        pltpu.VMEM(inverse.shape, F32),
+        dma((len(arrays) + 2,)),
         dma((T,)), dma((T,)), dma((T,)), dma((T,)), dma((T,)), dma((T,)),
         dma, dma, dma, dma, dma, dma,
     ]
-    return pl.pallas_call(
+    normal = pl.pallas_call(
         functools.partial(kernel, K, T),
-        out_shape=jax.ShapeDtypeStruct((B, out_proj.shape[1]), BF16),
-        in_specs=[
-            pl.BlockSpec(memory_space=pltpu.SMEM),
-            pl.BlockSpec(memory_space=pltpu.VMEM),
-        ]
-        + [pl.BlockSpec(memory_space=pl.ANY)] * len(arrays),
+        out_shape=jax.ShapeDtypeStruct((B, out_proj.shape[1]), F32),
+        in_specs=[pl.BlockSpec(memory_space=pl.ANY)] * (len(arrays) + 2),
         out_specs=pl.BlockSpec(memory_space=pltpu.VMEM),
         scratch_shapes=scratch,
         compiler_params=pltpu.CompilerParams(collective_id=0, has_side_effects=True),
     )(lengths, jnp.asarray(inverse), *arrays)
+    return (normal * row(output_gain)).astype(BF16)
 
 
 def solution(mesh):

time: 28.2 us -> 27.4 us (0.972)
  other arithmetic: 0 us -> 1.25 us
  local copies, waits for them, and re-layouts: 1.26 us -> 0.01 us
  Pallas kernels: 26.7 us -> 26 us
    unnamed x1 -> x2, local copies, waits for them, and re-layouts: 1.26 us -> 0.01 us
    convert_element_type x0 -> x1, other arithmetic: none -> 1.25 us  [shards(): return (normal * row(output_gain)).astype(BF16)]
    pallas_call x1, Pallas kernels: 26.7 us -> 26 us  [shards(): pl.pallas_call(functools.partial(kernel, K, T), out_shape=jax.ShapeDtypeS...]
where the time goes in v2:
time: 27.4 us; the launch traced here: 27.2 us
  Pallas kernels  26 us (95%)
  other arithmetic  1.25 us (5%)
    pallas_call x1, Pallas kernels, shards(): pl.pallas_call(functools.partial(kernel, K, T), out_shape=jax.ShapeDtypeS...  26 us
    convert_element_type x1, other arithmetic, shards(): return (normal * row(output_gain)).astype(BF16)  1.25 us

profile of v2, /device:TPU:0, one launch (start us, length us, event | category | flops | bytes accessed | tf_op | source)
XLA Modules:
  0.0 27.2 jit_solution(6994377076171807737)
XLA Ops:
  0.0 0.0 copy-start
  0.0 26.0 %shard_map.163 = f32[8,64]{1,0:T(8,128)} custom-call(s32[8]{0:T(128)} %lengths_h.1, f32[1,64]{1,0:T(1,128)} %constant.2.clone.inverse_h, bf16[8,512]{1,0:T(8,128)(2,1)} %hidden_h.1, f32[1,512]{1,0:T(1,128)} %bitcast.19, bf16[512,256]{1,0:T(8,128)(2,1)} %dq_h.1, bf16[512,256]{1,0:T(8,128)(2,1)} %dl_h.1, bf16[64,512]{1,0:T(8,128)(2,1)} %bitcast.17, ...), custom_call_target="tpu_custom_call" | custom-call | tf_op jit(solution)/shard_map/pallas_call | solution.py:440
  26.0 0.0 copy-done
  26.0 1.3 %multiply_convert_fusion = bf16[8,64]{1,0:T(8,128)(2,1)} fusion(f32[8,64]{1,0:T(8,128)} %shard_map.163, f32[64]{0:T(128)S(1)} %copy-done), kind=kLoop, calls=%fused_computation | loop fusion | flops 1024 | bytes 3328 | tf_op jit(solution)/shard_map/convert_element_type | solution.py:448
Async XLA Ops:
  0.0 26.0 %copy-start = (f32[64]{0:T(128)S(1)}, f32[64]{0:T(128)}, u32[]{:S(2)}) copy-start(f32[64]{0:T(128)} %param.29) | copy-start | bytes 772
